TPU v7x, 32 devices: a whole 2x2x4 slice. The times are simulated.
32 devices in a mesh: rep: 2 (over x), fs: 8 (over z, y), tp: 2 (over core).
Axes of the slice: x: 2, y: 2, z: 4, core: 2. Of those that a mesh axis runs over, the one named last changes fastest.
Arguments:
- inputs: bfloat16 [8192, 2048], P(('rep', 'fs')), may hold values from -6 to 6
- gain: float32 [2048], replicated, may hold values from 0.1 to 1.9
- gate_weight: bfloat16 [2048, 3072], P('fs', 'tp'), may hold values from -0.125 to 0.125
- up_weight: bfloat16 [2048, 3072], P('fs', 'tp'), may hold values from -0.125 to 0.125
- down_weight: bfloat16 [2048, 3072], P('fs', 'tp'), may hold values from -0.109375 to 0.109375
- cotangent: bfloat16 [8192, 2048], P(('rep', 'fs')), may hold values from -6 to 6
Outputs:
- input_gradient: bfloat16 [8192, 2048], P(('rep', 'fs'))
- gain_gradient: float32 [2048], replicated
- d_down: float32 [2048, 3072], P('fs', 'tp')
All inputs are finite; a program needn't handle non-finite values.
Results may differ from a plain program's by a relative error of at most 0.014.
Values may be sent and summed in bfloat16 or wider, within the bound.
A program may use at most 128 MiB of HBM per device.

v0:
```python
import jax
import jax.numpy as jnp
from jax import lax
from jax.sharding import PartitionSpec as P

EPS = 1e-06


def local(inputs, gain, gate_weight, up_weight, down_weight, cotangent):
    single_precision = inputs.astype(jnp.float32)
    reciprocal_root_mean = lax.rsqrt(
        jnp.mean(single_precision * single_precision, axis=-1, keepdims=True) + EPS
    )
    unit_input = single_precision * reciprocal_root_mean
    normalized_input = (unit_input * gain).astype(jnp.bfloat16)
    row_count = inputs.shape[0]
    contract_cols = (((1,), (1,)), ((), ()))
    gate_full, up_full, down_full = (
        lax.all_gather(gate_weight, "fs", axis=0, tiled=True),
        lax.all_gather(up_weight, "fs", axis=0, tiled=True),
        lax.all_gather(down_weight, "fs", axis=0, tiled=True),
    )
    gate = jnp.dot(normalized_input, gate_full, preferred_element_type=jnp.float32)
    up_proj = jnp.dot(normalized_input, up_full, preferred_element_type=jnp.float32)
    down_sum = jnp.dot(cotangent, down_full, preferred_element_type=jnp.float32)
    gate_sig = jax.nn.sigmoid(gate)
    active = gate * gate_sig
    hidden = (active * up_proj).astype(jnp.bfloat16)
    d_hidden = 0.5 * down_sum
    d_gate = (d_hidden * up_proj * gate_sig * (1.0 + gate * (1.0 - gate_sig))).astype(jnp.bfloat16)
    d_up = (d_hidden * active).astype(jnp.bfloat16)
    partial_value = lax.dot_general(
        d_gate, gate_full, contract_cols, preferred_element_type=jnp.float32
    ) + lax.dot_general(d_up, up_full, contract_cols, preferred_element_type=jnp.float32)
    summed_units = lax.psum(partial_value.astype(jnp.bfloat16), "tp")
    normalized_gradient = summed_units.astype(jnp.float32)
    gain_gradient = lax.psum(jnp.sum(normalized_gradient * unit_input, axis=0), ("rep", "fs"))
    gain_scaled = gain * normalized_gradient
    mean_correction = jnp.mean(gain_scaled * unit_input, axis=-1, keepdims=True)
    input_gradient = (
        cotangent.astype(jnp.float32)
        + reciprocal_root_mean * (gain_scaled - unit_input * mean_correction)
    ).astype(jnp.bfloat16)
    contract_rows = (((0,), (0,)), ((), ()))
    width = cotangent.shape[1]
    groups_fs = lax.axis_size("fs")
    groups_rep = lax.axis_size("rep")
    sub_rows = width // (groups_fs * groups_rep)
    reordered = (
        cotangent.reshape(row_count, groups_fs, groups_rep, sub_rows)
        .transpose(0, 2, 1, 3)
        .reshape(row_count, width)
    )
    summed = lax.psum_scatter(
        0.5 * lax.dot_general(reordered, hidden, contract_rows, preferred_element_type=jnp.float32),
        ("rep", "fs"),
        scatter_dimension=0,
        tiled=True,
    )
    d_down = lax.all_gather(summed, "rep", axis=0, tiled=True)
    return (input_gradient, gain_gradient, d_down)


def solution(mesh):
    placed = (
        P(("rep", "fs"), None),
        P(),
        P("fs", "tp"),
        P("fs", "tp"),
        P("fs", "tp"),
        P(("rep", "fs"), None),
    )
    return jax.shard_map(
        local,
        mesh=mesh,
        in_specs=placed,
        out_specs=(P(("rep", "fs"), None), P(), P("fs", "tp")),
        check_vma=False,
    )
```

profile of v0, /device:TPU:0, one launch (start us, length us, event | category | flops | bytes accessed | tf_op | source)
XLA Modules:
  0.0 600.7 jit_solution(4841965839708579481)
XLA Ops:
  7.2 0.0 copy-start.1
  7.2 0.0 all-gather.9.cloned.1.call-start
  7.2 0.7 all-gather.9.cloned.1.call-update
  7.9 0.0 all-gather.7.cloned.1.call-start
  8.0 0.7 all-gather.7.cloned.1.call-update
  8.7 0.0 all-gather.5.cloned.1.call-start
  8.7 0.7 all-gather.5.cloned.1.call-update
  9.4 0.0 reduce-scatter.2.cloned.1.call-start
  9.4 0.0 copy-done.1
  9.5 2.5 copy.11
  12.0 0.0 copy-start
  12.0 0.0 copy-start.3
  12.0 3.3 copy.12
  15.2 0.0 copy-done
  15.2 0.5 fusion.9
  15.7 95.9 %all-gather.9.cloned.1.call-done = bf16[2048,1536]{1,0:T(8,128)(2,1)} async-done(((bf16[256,1536]{1,0:T(8,128)(2,1)}), bf16[2048,1536]{1,0:T(8,128)(2,1)}) %all-gather.9.cloned.1.call-update) | async-done | bytes 6291472 | tf_op jit(solution)/shard_map/all_gather | solution.py:19
  111.6 0.0 copy-done.3
  111.6 7.9 %fusion.14 = f32[512,1536]{1,0:T(8,128)} fusion(bf16[2048,1536]{1,0:T(8,128)(2,1)} %all-gather.9.cloned.1.call-done, bf16[512,2048]{1,0:T(8,128)(2,1)S(1)} %copy-done, f32[2048]{0:T(1024)S(1)} %copy-done.3, f32[512]{0:T(512)S(1)} %add_rsqrt_fusion), kind=kOutput, calls=%fused_computation.25 | convolution fusion | flops 3225419776 | bytes 11544576 | tf_op jit(solution)/shard_map/dot_general | solution.py:23
  119.5 91.2 %all-gather.7.cloned.1.call-done = bf16[2048,1536]{1,0:T(8,128)(2,1)} async-done(((bf16[256,1536]{1,0:T(8,128)(2,1)}), bf16[2048,1536]{1,0:T(8,128)(2,1)}) %all-gather.7.cloned.1.call-update) | async-done | bytes 6291472 | tf_op jit(solution)/shard_map/all_gather | solution.py:20
  210.7 0.0 copy-start.2
  210.7 0.0 copy-start.4
  210.7 5.8 fusion.16
  216.5 0.0 copy-start.6
  216.5 1.7 copy-done.6
  218.2 0.0 copy-done.2
  218.2 0.0 copy-done.4
  218.2 6.8 %multiply_bitcast_fusion = f32[2048,1536]{0,1:T(8,128)} fusion(bf16[512,2048]{0,1:T(8,128)(2,1)S(1)} %bitcast.14, f32[512,1536]{1,0:T(8,128)S(1)} %fusion.16, f32[512,1536]{1,0:T(8,128)S(1)} %copy-done.4), kind=kOutput, calls=%fused_computation | convolution fusion | flops 3229089792 | bytes 20971520 | tf_op jit(solution)/shard_map/dot_general | solution.py:55
  225.1 0.0 reduce-scatter.2.cloned.1.call-update
  225.1 0.2 all-reduce.2.cloned.1.call-start
  225.3 84.5 %all-gather.5.cloned.1.call-done = bf16[2048,1536]{1,0:T(8,128)(2,1)} async-done(((bf16[256,1536]{1,0:T(8,128)(2,1)}), bf16[2048,1536]{1,0:T(8,128)(2,1)}) %all-gather.5.cloned.1.call-update) | async-done | bytes 6291472 | tf_op jit(solution)/shard_map/all_gather | solution.py:21
  309.8 0.0 copy-start.5
  309.8 0.0 slice-start
  309.8 8.6 %convolution_multiply_fusion = f32[512,1536]{1,0:T(8,128)} fusion(bf16[512,2048]{1,0:T(8,128)(2,1)} %param.11, bf16[2048,1536]{1,0:T(8,128)(2,1)} %all-gather.5.cloned.1.call-done), kind=kOutput, calls=%fused_computation.17 | convolution fusion | flops 3222011904 | bytes 11534336 | tf_op jit(solution)/shard_map/dot_general | solution.py:25
  318.4 0.0 copy-done.5
  318.4 0.0 copy-done.7
  318.4 8.6 %fusion.12 = f32[512,2048]{1,0:T(8,128)S(1)} fusion(bf16[2048,1536]{1,0:T(8,128)(2,1)} %all-gather.9.cloned.1.call-done, f32[512,1536]{1,0:T(8,128)S(1)} %copy-done.5, f32[512,1536]{1,0:T(8,128)} %convolution_multiply_fusion, f32[512,1536]{1,0:T(8,128)S(1)} %copy-done.7), kind=kOutput, calls=%fused_computation.23 | convolution fusion | flops 3229089792 | bytes 19922944 | tf_op jit(solution)/shard_map/dot_general | solution.py:32
  327.0 0.0 slice-done
  327.0 0.0 slice-done.1
  327.1 6.6 %add_convert_fusion = bf16[512,2048]{1,0:T(8,128)(2,1)} fusion(f32[512,2048]{1,0:T(8,128)S(1)} %fusion.12, bf16[2048,1536]{1,0:T(8,128)(2,1)S(1)} %bitcast.16, f32[512,1536]{1,0:T(8,128)} %convolution_multiply_fusion, f32[512,1536]{1,0:T(8,128)S(1)} %copy-done.5), kind=kOutput, calls=%fused_computation.16 | convolution fusion | flops 3228041216 | bytes 18874368 | tf_op jit(solution)/shard_map/dot_general | solution.py:34
  333.7 0.0 all-reduce.2.cloned.1.call-update
  333.7 0.0 all-gather.11.cloned.1.call-start
  333.7 182.3 %reduce-scatter.2.cloned.1.call-done = f32[128,1536]{0,1:T(8,128)} async-done(((f32[2048,1536]{0,1:T(8,128)}), f32[128,1536]{0,1:T(8,128)}) %reduce-scatter.2.cloned.1.call-update) | async-done | bytes 786448 | tf_op jit(solution)/shard_map/reduce_scatter | solution.py:54
  516.0 0.0 all-gather.11.cloned.1.call-update
  516.1 23.6 %all-reduce.2.cloned.1.call-done = bf16[512,2048]{1,0:T(8,128)(2,1)} async-done(((bf16[512,2048]{1,0:T(8,128)(2,1)}), bf16[512,2048]{1,0:T(8,128)(2,1)}) %all-reduce.2.cloned.1.call-update) | async-done | bytes 2097168 | tf_op jit(solution)/shard_map/psum | solution.py:35
  539.6 2.9 fusion.10
  542.5 43.3 %psum.15 = f32[2048]{0:T(1024)} all-reduce(f32[2048]{0:T(1024)S(1)} %get-tuple-element.12), channel_id=1, replica_groups=mesh['rep'=2,'fs'=8,'tp'=2] {'rep','fs'}, use_global_device_ids=true, to_apply=%region_4.0 | all-reduce | flops 2048 | bytes 16384 | tf_op jit(solution)/shard_map/psum | solution.py:37
  585.8 5.0 fusion.6
  590.8 3.0 copy.13
  (6 shorter events, 0.0 us)
Async XLA Ops:
  7.2 2.3 copy-start.1
  7.2 104.4 %all-gather.9.cloned.1.call-start = ((), (), s32[]{:S(2)}) async-start(), calls=%async_computation.3 | async-start | bytes 7077888 | tf_op jit(solution)/shard_map/all_gather | solution.py:19
  7.9 202.8 %all-gather.7.cloned.1.call-start = ((), (), s32[]{:S(2)}) async-start(), calls=%async_computation.2 | async-start | bytes 7077888 | tf_op jit(solution)/shard_map/all_gather | solution.py:20
  8.7 301.1 %all-gather.5.cloned.1.call-start = ((), (), s32[]{:S(2)}) async-start(), calls=%async_computation.1 | async-start | bytes 7077888 | tf_op jit(solution)/shard_map/all_gather | solution.py:21
  9.4 506.6 %reduce-scatter.2.cloned.1.call-start = ((), (), s32[]{:S(2)}) async-start(), calls=%async_computation.5 | async-start | bytes 13369344 | tf_op jit(solution)/shard_map/reduce_scatter | solution.py:54
  12.0 3.3 copy-start
  12.0 99.7 %copy-start.3 = (f32[2048]{0:T(1024)S(1)}, f32[2048]{0:T(1024)}, u32[]{:S(2)}) copy-start(f32[2048]{0:T(1024)} %param.7) | copy-start | bytes 24580
  210.7 7.5 %copy-start.2 = (bf16[512,2,8,128]{0,3,2,1:T(8,128)(2,1)S(1)}, bf16[512,2,8,128]{0,3,2,1:T(8,128)(2,1)}, u32[]{:S(2)}) copy-start(bf16[512,2,8,128]{0,3,2,1:T(8,128)(2,1)} %copy.12) | copy-start | bytes 6291460
  210.7 7.5 %copy-start.4 = (f32[512,1536]{1,0:T(8,128)S(1)}, f32[512,1536]{1,0:T(8,128)}, u32[]{:S(2)}) copy-start(f32[512,1536]{1,0:T(8,128)} %fusion.14) | copy-start | bytes 9437188
  216.5 1.8 copy-start.6
  225.1 314.5 %all-reduce.2.cloned.1.call-start = ((), (), s32[]{:S(2)}) async-start(), calls=%async_computation.4 | async-start | bytes 4194304 | tf_op jit(solution)/shard_map/psum | solution.py:35
  309.8 8.6 %copy-start.5 = (f32[512,1536]{1,0:T(8,128)S(1)}, f32[512,1536]{1,0:T(8,128)}, u32[]{:S(2)}) copy-start(f32[512,1536]{1,0:T(8,128)} %fusion.14) | copy-start | bytes 9437188
  309.8 8.6 %copy-start.7 = (f32[512,1536]{1,0:T(8,128)S(1)}, f32[512,1536]{1,0:T(8,128)}, u32[]{:S(2)}) copy-start(f32[512,1536]{1,0:T(8,128)} %copy-done.6) | copy-start | bytes 9437188
  309.8 17.2 %slice-start = ((s8[6291456]{0:T(1024)(128)(4,1)}), s8[4194304]{0:T(1024)(128)(4,1)S(1)}, s32[]{:S(2)}) async-start(s8[6291456]{0:T(1024)(128)(4,1)} %bitcast.15), calls=%async_computation.7 | async-start | bytes 8388608
  318.4 8.6 %slice-start.1 = ((s8[6291456]{0:T(1024)(128)(4,1)}), s8[2097152]{0:T(1024)(128)(4,1)S(1)}, s32[]{:S(2)}) async-start(s8[6291456]{0:T(1024)(128)(4,1)} %bitcast.15), calls=%async_computation.8 | async-start | bytes 4194304
  333.7 257.1 %all-gather.11.cloned.1.call-start = ((), (), s32[]{:S(2)}) async-start(), calls=%async_computation.6 | async-start | bytes 2359296 | tf_op jit(solution)/shard_map/all_gather | solution.py:60
Sparse Core Ops, SparseCore 0:
  10.2 101.4 all-gather.8
  113.8 96.8 all-gather.6
  212.9 96.8 all-gather.4
  315.3 200.6 reduce-scatter.1
  518.8 20.7 all-reduce.1
  541.0 28.3 all-gather.10
where the time goes:
time: 601 us
  waiting for transfers between devices  480 us (80%)
  matrix products  44.2 us (7%)
  blocking collectives  43.3 us (7%)
  between operations  14.2 us (2%)
  local copies, waits for them, and re-layouts  10.6 us (2%)
  other arithmetic  8.39 us (1%)
    reduce_scatter x1, waiting for transfers between devices, local(): lax.psum_scatter(0.5 * lax.dot_general(reordered, hidden, contract_rows,...  182 us
    all_gather x1, waiting for transfers between devices, local(): lax.all_gather(gate_weight, 'fs', axis=0, tiled=True)  95.9 us
    all_gather x1, waiting for transfers between devices, local(): lax.all_gather(up_weight, 'fs', axis=0, tiled=True)  91.2 us
    all_gather x1, waiting for transfers between devices, local(): lax.all_gather(down_weight, 'fs', axis=0, tiled=True)  84.5 us
    psum x1, blocking collectives, local(): lax.psum(jnp.sum(normalized_gradient * unit_input, axis=0), ('rep', 'fs'))  43.3 us
    psum x1, waiting for transfers between devices, local(): summed_units = lax.psum(partial_value.astype(jnp.bfloat16), 'tp')  23.6 us
  transfers between devices with their start and end apart: 6, of which 5 were waited for; matrix products, arithmetic and copies ran while one was open for 10% of the time, Pallas kernels for 0%

commit v1 on v0

--- a/solution.py
+++ b/solution.py
@@ -4,6 +4,28 @@
 from jax.sharding import PartitionSpec as P
 
 EPS = 1e-06
+
+
+def laid_out(blocks, dim):
+    shape = list(blocks.shape[1:])
+    shape[dim] *= blocks.shape[0]
+    return jnp.moveaxis(blocks, 0, dim).reshape(shape)
+
+
+def collected_by_bits(value, axis):
+    size = lax.axis_size(axis)
+    blocks = value[None]
+    for level in range(size.bit_length() - 1):
+        bit = 1 << level
+        received = lax.ppermute(blocks, axis, [(i, i ^ bit) for i in range(size)])
+        both = jnp.stack([blocks, received])
+        upper = lax.axis_index(axis) >> level & 1
+        blocks = jnp.where(upper == 0, both, both[::-1]).reshape(-1, *value.shape)
+    return blocks
+
+
+def gather_by_bits(x, axis, dim):
+    return laid_out(collected_by_bits(x, axis), dim)
 
 
 def local(inputs, gain, gate_weight, up_weight, down_weight, cotangent):
@@ -17,7 +39,7 @@
     contract_cols = (((1,), (1,)), ((), ()))
     gate_full, up_full, down_full = (
         lax.all_gather(gate_weight, "fs", axis=0, tiled=True),
-        lax.all_gather(up_weight, "fs", axis=0, tiled=True),
+        gather_by_bits(up_weight, "fs", 0),
         lax.all_gather(down_weight, "fs", axis=0, tiled=True),
     )
     gate = jnp.dot(normalized_input, gate_full, preferred_element_type=jnp.float32)

time: 601 us -> 656 us (1.092)
  waiting for transfers between devices: 480 us -> 519 us
  other arithmetic: 8.39 us -> 18.8 us
    ppermute x0 -> x3, waiting for transfers between devices: none -> 316 us  [collected_by_bits(): received = lax.ppermute(blocks, axis, [(i, i ^ bit) for i in range(size)])]
    all_gather x1, waiting for transfers between devices: 95.9 us -> 0.01 us  [local(): lax.all_gather(gate_weight, 'fs', axis=0, tiled=True)]
    all_gather x1 -> x0, waiting for transfers between devices: 91.2 us -> none  [local(): lax.all_gather(up_weight, 'fs', axis=0, tiled=True)]
    all_gather x1, waiting for transfers between devices: 84.5 us -> 0.02 us  [local(): lax.all_gather(down_weight, 'fs', axis=0, tiled=True)]
    another operation x0 -> x4, other arithmetic: none -> 6.79 us  [collected_by_bits(): both = jnp.stack([blocks, received])]
  transfers between devices with their start and end apart: 6 -> 8, of which waited for: 5 -> 5; matrix products, arithmetic and copies ran while one was open for 10% -> 10% of each run, Pallas kernels for 0% -> 0%
where the time goes in v1:
time: 656 us
  waiting for transfers between devices  519 us (79%)
  blocking collectives  43.3 us (7%)
  matrix products  41.6 us (6%)
  other arithmetic  18.8 us (3%)
  between operations  13.9 us (2%)
  local copies, waits for them, and re-layouts  13.1 us (2%)
    ppermute x3, waiting for transfers between devices, collected_by_bits(): received = lax.ppermute(blocks, axis, [(i, i ^ bit) for i in range(size)])  316 us
    reduce_scatter x1, waiting for transfers between devices, local(): lax.psum_scatter(0.5 * lax.dot_general(reordered, hidden, contract_rows,...  179 us
    psum x1, blocking collectives, local(): lax.psum(jnp.sum(normalized_gradient * unit_input, axis=0), ('rep', 'fs'))  43.3 us
    psum x1, waiting for transfers between devices, local(): summed_units = lax.psum(partial_value.astype(jnp.bfloat16), 'tp')  23.6 us
  transfers between devices with their start and end apart: 8, of which 5 were waited for; matrix products, arithmetic and copies ran while one was open for 10% of the time, Pallas kernels for 0%

profile of v1, /device:TPU:0, one launch (start us, length us, event | category | flops | bytes accessed | tf_op | source)
XLA Modules:
  0.0 656.0 jit_solution(15803119656773421328)
XLA Ops:
  7.2 0.0 all-gather.6.cloned.1.call-start
  7.2 0.7 all-gather.6.cloned.1.call-update
  7.9 0.0 all-gather.4.cloned.1.call-start
  7.9 3.1 collective-permute-start
  11.0 0.0 all-gather.4.cloned.1.call-update
  11.0 0.0 reduce-scatter.2.cloned.1.call-start
  11.1 24.5 %collective-permute-done = bf16[1,256,1536]{2,1,0:T(8,128)(2,1)S(1)} collective-permute-done((bf16[1,256,1536]{2,1,0:T(8,128)(2,1)}, bf16[1,256,1536]{2,1,0:T(8,128)(2,1)S(1)}, u32[]{:S(2)}, u32[]{:S(2)}) %collective-permute-start) | collective-permute-done | bytes 786464 | tf_op jit(solution)/shard_map/ppermute | solution.py:20
  35.6 1.3 pad_maximum_fusion.2
  36.9 0.4 fusion.15
  37.3 1.5 collective-permute-start.1
  38.7 85.5 %collective-permute-done.1 = bf16[2,256,1536]{2,1,0:T(8,128)(2,1)} collective-permute-done((bf16[2,256,1536]{2,1,0:T(8,128)(2,1)S(1)}, bf16[2,256,1536]{2,1,0:T(8,128)(2,1)}, u32[]{:S(2)}, u32[]{:S(2)}) %collective-permute-start.1) | collective-permute-done | bytes 1572896 | tf_op jit(solution)/shard_map/ppermute | solution.py:20
  124.2 1.7 pad_maximum_fusion.1
  126.0 0.0 copy-start.1
  126.0 2.3 reverse_select_fusion.1
  128.2 0.9 collective-permute-start.2
  129.2 0.0 copy-done.1
  129.2 2.5 copy.11
  131.7 3.3 copy.12
  134.9 0.0 copy-done
  134.9 0.5 fusion.9
  135.4 205.8 %collective-permute-done.2 = bf16[4,256,1536]{2,1,0:T(8,128)(2,1)} collective-permute-done((bf16[4,256,1536]{2,1,0:T(8,128)(2,1)}, bf16[4,256,1536]{2,1,0:T(8,128)(2,1)}, u32[]{:S(2)}, u32[]{:S(2)}) %collective-permute-start.2) | collective-permute-done | bytes 3145760 | tf_op jit(solution)/shard_map/ppermute | solution.py:20
  341.2 3.4 pad_maximum_fusion
  344.6 0.0 copy-start.4
  344.6 1.3 reverse_select_fusion
  346.0 0.0 copy-start.2
  346.0 2.7 copy-done.2
  348.7 0.0 copy-done.4
  348.7 5.2 fusion.18
  353.9 5.8 fusion.16
  359.6 1.6 copy-done.7
  361.2 7.0 %multiply_bitcast_fusion = f32[2048,1536]{0,1:T(8,128)} fusion(bf16[512,2048]{0,1:T(8,128)(2,1)S(1)} %bitcast.30, f32[512,1536]{1,0:T(8,128)S(1)} %copy-done.5, f32[512,1536]{1,0:T(8,128)S(1)} %fusion.16), kind=kOutput, calls=%fused_computation | convolution fusion | flops 3229089792 | bytes 20971520 | tf_op jit(solution)/shard_map/dot_general | solution.py:77
  368.2 0.0 reduce-scatter.2.cloned.1.call-update
  368.2 0.2 all-reduce.2.cloned.1.call-start
  368.5 0.0 all-gather.4.cloned.1.call-done
  368.5 0.0 slice-start
  368.5 8.6 %convolution_multiply_fusion = f32[512,1536]{1,0:T(8,128)} fusion(bf16[512,2048]{1,0:T(8,128)(2,1)} %param.11, bf16[2048,1536]{1,0:T(8,128)(2,1)} %all-gather.4.cloned.1.call-done), kind=kOutput, calls=%fused_computation.20 | convolution fusion | flops 3222011904 | bytes 11534336 | tf_op jit(solution)/shard_map/dot_general | solution.py:47
  377.1 0.0 copy-done.6
  377.1 8.5 %fusion.12 = f32[512,2048]{1,0:T(8,128)S(1)} fusion(bf16[2048,1536]{1,0:T(8,128)(2,1)} %all-gather.6.cloned.1.call-done, f32[512,1536]{1,0:T(8,128)S(1)} %copy-done.8, f32[512,1536]{1,0:T(8,128)} %convolution_multiply_fusion, f32[512,1536]{1,0:T(8,128)S(1)} %copy-done.6), kind=kOutput, calls=%fused_computation.28 | convolution fusion | flops 3229089792 | bytes 19922944 | tf_op jit(solution)/shard_map/dot_general | solution.py:54
  385.7 6.6 %add_convert_fusion = bf16[512,2048]{1,0:T(8,128)(2,1)} fusion(f32[512,2048]{1,0:T(8,128)S(1)} %fusion.12, bf16[2048,1536]{1,0:T(8,128)(2,1)S(1)} %bitcast.29, f32[512,1536]{1,0:T(8,128)} %convolution_multiply_fusion, f32[512,1536]{1,0:T(8,128)S(1)} %copy-done.8), kind=kOutput, calls=%fused_computation.19 | convolution fusion | flops 3228041216 | bytes 18874368 | tf_op jit(solution)/shard_map/dot_general | solution.py:56
  392.3 0.0 all-reduce.2.cloned.1.call-update
  392.3 0.0 all-gather.8.cloned.1.call-start
  392.4 179.2 %reduce-scatter.2.cloned.1.call-done = f32[128,1536]{0,1:T(8,128)} async-done(((f32[2048,1536]{0,1:T(8,128)}), f32[128,1536]{0,1:T(8,128)}) %reduce-scatter.2.cloned.1.call-update) | async-done | bytes 786448 | tf_op jit(solution)/shard_map/reduce_scatter | solution.py:76
  571.6 0.0 all-gather.8.cloned.1.call-update
  571.6 23.6 %all-reduce.2.cloned.1.call-done = bf16[512,2048]{1,0:T(8,128)(2,1)} async-done(((bf16[512,2048]{1,0:T(8,128)(2,1)}), bf16[512,2048]{1,0:T(8,128)(2,1)}) %all-reduce.2.cloned.1.call-update) | async-done | bytes 2097168 | tf_op jit(solution)/shard_map/psum | solution.py:57
  595.2 2.9 fusion.10
  598.1 43.3 %psum.15 = f32[2048]{0:T(1024)} all-reduce(f32[2048]{0:T(1024)S(1)} %get-tuple-element.12), channel_id=1, replica_groups=mesh['rep'=2,'fs'=8,'tp'=2] {'rep','fs'}, use_global_device_ids=true, to_apply=%region_4.5 | all-reduce | flops 2048 | bytes 16384 | tf_op jit(solution)/shard_map/psum | solution.py:59
  641.4 5.0 fusion.6
  646.4 3.0 copy.13
  (17 shorter events, 0.0 us)
Async XLA Ops:
  7.2 346.7 %all-gather.6.cloned.1.call-start = ((), (), s32[]{:S(2)}) async-start(), calls=%async_computation.2 | async-start | bytes 7077888 | tf_op jit(solution)/shard_map/all_gather | solution.py:41
  7.9 360.6 %all-gather.4.cloned.1.call-start = ((), (), s32[]{:S(2)}) async-start(), calls=%async_computation.1 | async-start | bytes 7077888 | tf_op jit(solution)/shard_map/all_gather | solution.py:43
  7.9 27.7 %collective-permute-start = (bf16[1,256,1536]{2,1,0:T(8,128)(2,1)}, bf16[1,256,1536]{2,1,0:T(8,128)(2,1)S(1)}, u32[]{:S(2)}, u32[]{:S(2)}) collective-permute-start(bf16[1,256,1536]{2,1,0:T(8,128)(2,1)} %bitcast.31), channel_id=1, source_target_pairs={{0,2},{2,0},{4,6},{6,4},{8,10},{10,8},{12,14},{14,12},{1,3},{3,1},... | collective-permute-start | bytes 2359304 | tf_op jit(solution)/shard_map/ppermute | solution.py:20
  11.0 560.5 %reduce-scatter.2.cloned.1.call-start = ((), (), s32[]{:S(2)}) async-start(), calls=%async_computation.4 | async-start | bytes 13369344 | tf_op jit(solution)/shard_map/reduce_scatter | solution.py:76
  37.3 87.0 %collective-permute-start.1 = (bf16[2,256,1536]{2,1,0:T(8,128)(2,1)S(1)}, bf16[2,256,1536]{2,1,0:T(8,128)(2,1)}, u32[]{:S(2)}, u32[]{:S(2)}) collective-permute-start(bf16[2,256,1536]{2,1,0:T(8,128)(2,1)S(1)} %get-tuple-element.15), channel_id=1, source_target_pairs={{0,4},{2,6},{4,0},{6,2},{8,12},{10,14},{12,8},{14,10},{1,5},{3,7},... | collective-permute-start | bytes 4718600 | tf_op jit(solution)/shard_map/ppermute | solution.py:20
  126.0 3.2 copy-start.1
  128.2 212.9 %collective-permute-start.2 = (bf16[4,256,1536]{2,1,0:T(8,128)(2,1)}, bf16[4,256,1536]{2,1,0:T(8,128)(2,1)}, u32[]{:S(2)}, u32[]{:S(2)}) collective-permute-start(bf16[4,256,1536]{2,1,0:T(8,128)(2,1)} %bitcast.7), channel_id=1, source_target_pairs={{0,8},{2,10},{4,12},{6,14},{8,0},{10,2},{12,4},{14,6},{1,9},{3,11}... | collective-permute-start | bytes 9437192 | tf_op jit(solution)/shard_map/ppermute | solution.py:20
  131.7 3.3 copy-start
  344.6 4.1 copy-start.4
  346.0 2.7 copy-start.2
  353.9 7.4 %copy-start.3 = (bf16[512,2,8,128]{0,3,2,1:T(8,128)(2,1)S(1)}, bf16[512,2,8,128]{0,3,2,1:T(8,128)(2,1)}, u32[]{:S(2)}) copy-start(bf16[512,2,8,128]{0,3,2,1:T(8,128)(2,1)} %copy.12) | copy-start | bytes 6291460
  353.9 7.4 %copy-start.5 = (f32[512,1536]{1,0:T(8,128)S(1)}, f32[512,1536]{1,0:T(8,128)}, u32[]{:S(2)}) copy-start(f32[512,1536]{1,0:T(8,128)} %fusion.18) | copy-start | bytes 9437188
  359.6 1.6 copy-start.7
  368.2 227.0 %all-reduce.2.cloned.1.call-start = ((), (), s32[]{:S(2)}) async-start(), calls=%async_computation.3 | async-start | bytes 4194304 | tf_op jit(solution)/shard_map/psum | solution.py:57
  368.5 8.6 %copy-start.6 = (f32[512,1536]{1,0:T(8,128)S(1)}, f32[512,1536]{1,0:T(8,128)}, u32[]{:S(2)}) copy-start(f32[512,1536]{1,0:T(8,128)} %fusion.18) | copy-start | bytes 9437188
  368.5 8.6 %copy-start.8 = (f32[512,1536]{1,0:T(8,128)S(1)}, f32[512,1536]{1,0:T(8,128)}, u32[]{:S(2)}) copy-start(f32[512,1536]{1,0:T(8,128)} %copy-done.7) | copy-start | bytes 9437188
  368.5 17.2 %slice-start = ((s8[6291456]{0:T(1024)(128)(4,1)}), s8[4194304]{0:T(1024)(128)(4,1)S(1)}, s32[]{:S(2)}) async-start(s8[6291456]{0:T(1024)(128)(4,1)} %bitcast.27), calls=%async_computation.6 | async-start | bytes 8388608
  377.1 8.6 %slice-start.1 = ((s8[6291456]{0:T(1024)(128)(4,1)}), s8[2097152]{0:T(1024)(128)(4,1)S(1)}, s32[]{:S(2)}) async-start(s8[6291456]{0:T(1024)(128)(4,1)} %bitcast.27), calls=%async_computation.7 | async-start | bytes 4194304
  392.3 254.1 %all-gather.8.cloned.1.call-start = ((), (), s32[]{:S(2)}) async-start(), calls=%async_computation.5 | async-start | bytes 2359296 | tf_op jit(solution)/shard_map/all_gather | solution.py:82
Sparse Core Ops, SparseCore 0:
  10.2 130.0 all-gather.5
  142.4 183.2 all-gather.3
  368.3 203.1 reduce-scatter.1
  574.3 20.7 all-reduce.1
  596.6 28.3 all-gather.7
